TPU v7x, 32 devices: a whole 2x2x4 slice. The times are simulated.
32 devices in a mesh: grp: 2 (over y), ra: 4 (over z), cb: 2 (over x), dp: 2 (over core).
Axes of the slice: x: 2, y: 2, z: 4, core: 2. Of those that a mesh axis runs over, the one named last changes fastest.
Arguments:
- tokens: bfloat16 [256, 2048], P(('grp', 'dp'), 'ra'), parts along dimension 0, may hold values from -62 to 62
- gain_first: float32 [2048], P('ra'), may hold values from 0.1 to 1.9
- up_first: bfloat16 [2048, 8192], P('ra', 'cb'), may hold values from -0.125 to 0.125
- down_first: bfloat16 [8192, 2048], P('cb', 'ra'), may hold values from -0.0625 to 0.0625
- gain_second: float32 [2048], P('ra'), may hold values from 0.1 to 1.9
- up_second: bfloat16 [2048, 8192], P('ra', 'cb'), may hold values from -0.125 to 0.125
- down_second: bfloat16 [8192, 2048], P('cb', 'ra'), may hold values from -0.0625 to 0.0625
- gain_last: float32 [2048], P('ra'), may hold values from 0.1 to 1.9
Outputs:
- normed: bfloat16 [256, 2048], P(('grp', 'dp'), 'ra'), parts along dimension 0
There are 2 independent parts, one for each index of `grp`. A program takes and returns all parts, laid end to end along the dimension named above; an argument that names none is the same for every part. Nothing has to cross between parts.
All inputs are finite; a program needn't handle non-finite values.
Results may differ from a plain program's by a relative error of at most 0.0095.
Values may be sent and summed in bfloat16 or wider, within the bound.
A program may use at most 64 MiB of HBM per device.

v0:
```python
import jax
import jax.numpy as jnp
from jax import lax
from jax.sharding import PartitionSpec as P

D = 2048
EPS = 1e-06


def squares_inverse(h32):
    local_sq = jnp.sum(h32 * h32, axis=1)
    summed_sq = lax.psum(local_sq, "ra")
    return lax.rsqrt(summed_sq / D + EPS)


def activate(summed, inverse):
    return jnp.square(jax.nn.relu(summed * inverse[:, None])).astype(jnp.bfloat16)


def mlp_branch(h32, gain, w_up, w_down):
    scaled = (h32 * gain).astype(jnp.bfloat16)
    partial_value = jnp.dot(scaled, w_up, preferred_element_type=jnp.float32)
    inverse = squares_inverse(h32)
    shared = lax.psum_scatter(partial_value, "ra", scatter_dimension=1, tiled=True)
    hidden_share = activate(shared, inverse)
    down = jnp.dot(
        lax.all_gather(hidden_share, "ra", axis=1, tiled=True),
        w_down,
        preferred_element_type=jnp.float32,
    )
    return lax.psum(down, "cb")


def local(tokens, gain_first, up_first, down_first, gain_second, up_second, down_second, gain_last):
    start32 = tokens.astype(jnp.float32)
    first = (0.5 * start32 + mlp_branch(start32, gain_first, up_first, down_first)).astype(
        jnp.bfloat16
    )
    first32 = first.astype(jnp.float32)
    second = (0.5 * first32 + mlp_branch(first32, gain_second, up_second, down_second)).astype(
        jnp.bfloat16
    )
    second32 = second.astype(jnp.float32)
    inverse = squares_inverse(second32)
    return (second32 * inverse[:, None] * gain_last).astype(jnp.bfloat16)


def solution(mesh):
    return jax.shard_map(
        local,
        mesh=mesh,
        in_specs=(
            P(("grp", "dp"), "ra"),
            P("ra"),
            P("ra", "cb"),
            P("cb", "ra"),
            P("ra"),
            P("ra", "cb"),
            P("cb", "ra"),
            P("ra"),
        ),
        out_specs=P(("grp", "dp"), "ra"),
        check_vma=False,
    )
```

profile of v0, /device:TPU:0, one launch (start us, length us, event | category | flops | bytes accessed | tf_op | source)
XLA Modules:
  0.0 175.9 jit_solution(10254012345547402609)
XLA Ops:
  6.5 0.0 copy-start
  6.5 0.0 reduce-scatter.3.cloned.1.call-start
  6.5 4.1 %fusion.13 = f32[64,4096]{1,0:T(8,128)} fusion(bf16[512,4096]{1,0:T(8,128)(2,1)} %param.10, bf16[64,512]{1,0:T(8,128)(2,1)} %param.8, f32[512]{0:T(512)} %param.9), kind=kOutput, calls=%fused_computation.22 | convolution fusion | flops 268533760 | bytes 5310464 | tf_op jit(solution)/shard_map/dot_general | solution.py:22
  10.6 0.0 copy-start.1
  10.7 0.0 reduce-scatter.3.cloned.1.call-update
  10.7 0.0 all-reduce.3.cloned.1.call-start
  10.7 0.0 copy-done
  10.7 0.1 fusion.6
  10.8 13.5 %psum.35 = f32[64]{0:T(128)S(1)} all-reduce(f32[64]{0:T(128)S(1)} %fusion.6), channel_id=1, replica_groups=mesh['grp'=2,'ra'=4,'cb'=2,'dp'=2] {'ra'}, use_global_device_ids=true, to_apply=%region_2.0 | all-reduce | flops 64 | bytes 512 | tf_op jit(solution)/shard_map/psum | solution.py:12
  24.4 16.5 %reduce-scatter.3.cloned.1.call-done = f32[64,1024]{1,0:T(8,128)} async-done(((f32[64,4096]{1,0:T(8,128)}), f32[64,1024]{1,0:T(8,128)}) %reduce-scatter.3.cloned.1.call-update) | async-done | bytes 262160 | tf_op jit(solution)/shard_map/reduce_scatter | solution.py:24
  40.9 1.0 multiply_convert_fusion.1
  41.9 15.9 %all_gather.6 = bf16[64,4096]{1,0:T(8,128)(2,1)S(1)} all-gather(bf16[64,1024]{1,0:T(8,128)(2,1)S(1)} %multiply_convert_fusion.1), channel_id=1, replica_groups=mesh['grp'=2,'ra'=4,'cb'=2,'dp'=2] {'ra'}, dimensions={1}, use_global_device_ids=true | all-gather | bytes 655360 | tf_op jit(solution)/shard_map/all_gather | solution.py:27
  57.8 3.7 %fusion.18 = f32[64,512]{1,0:T(8,128)} fusion(bf16[64,4096]{1,0:T(8,128)(2,1)S(1)} %all_gather.6, bf16[4096,512]{1,0:T(8,128)(2,1)} %param.11), kind=kOutput, calls=%fused_computation.28 | convolution fusion | flops 268435456 | bytes 4849664 | tf_op jit(solution)/shard_map/dot_general | solution.py:26
  61.5 0.0 all-reduce.3.cloned.1.call-update
  61.5 0.0 reduce-scatter.5.cloned.1.call-start
  61.6 20.1 %all-reduce.3.cloned.1.call-done = f32[64,512]{1,0:T(8,128)} async-done(((f32[64,512]{1,0:T(8,128)}), f32[64,512]{1,0:T(8,128)}) %all-reduce.3.cloned.1.call-update) | async-done | bytes 131088 | tf_op jit(solution)/shard_map/psum | solution.py:31
  81.7 1.0 fusion.10
  82.7 0.0 copy-done.1
  82.7 4.0 %fusion.11 = f32[64,4096]{1,0:T(8,128)} fusion(bf16[512,4096]{1,0:T(8,128)(2,1)} %param.13, bf16[64,512]{1,0:T(8,128)(2,1)S(1)} %get-tuple-element.6, f32[512]{0:T(512)S(1)} %copy-done.1), kind=kOutput, calls=%fused_computation.21 | convolution fusion | flops 268533760 | bytes 5310464 | tf_op jit(solution)/shard_map/dot_general | solution.py:22
  86.7 0.0 copy-start.2
  86.7 0.0 reduce-scatter.5.cloned.1.call-update
  86.8 0.0 all-reduce.5.cloned.1.call-start
  86.8 11.9 %psum.37 = f32[64]{0:T(128)S(1)} all-reduce(f32[64]{0:T(128)S(1)} %get-tuple-element.5), channel_id=1, replica_groups=mesh['grp'=2,'ra'=4,'cb'=2,'dp'=2] {'ra'}, use_global_device_ids=true, to_apply=%region_6.7 | all-reduce | flops 64 | bytes 512 | tf_op jit(solution)/shard_map/psum | solution.py:12
  98.7 15.6 %reduce-scatter.5.cloned.1.call-done = f32[64,1024]{1,0:T(8,128)} async-done(((f32[64,4096]{1,0:T(8,128)}), f32[64,1024]{1,0:T(8,128)}) %reduce-scatter.5.cloned.1.call-update) | async-done | bytes 262160 | tf_op jit(solution)/shard_map/reduce_scatter | solution.py:24
  114.3 1.0 multiply_convert_fusion
  115.3 15.9 %all_gather.7 = bf16[64,4096]{1,0:T(8,128)(2,1)S(1)} all-gather(bf16[64,1024]{1,0:T(8,128)(2,1)S(1)} %multiply_convert_fusion), channel_id=1, replica_groups=mesh['grp'=2,'ra'=4,'cb'=2,'dp'=2] {'ra'}, dimensions={1}, use_global_device_ids=true | all-gather | bytes 655360 | tf_op jit(solution)/shard_map/all_gather | solution.py:27
  131.2 3.7 %fusion.19 = f32[64,512]{1,0:T(8,128)} fusion(bf16[64,4096]{1,0:T(8,128)(2,1)S(1)} %all_gather.7, bf16[4096,512]{1,0:T(8,128)(2,1)} %param.14), kind=kOutput, calls=%fused_computation.29 | convolution fusion | flops 268435456 | bytes 4849664 | tf_op jit(solution)/shard_map/dot_general | solution.py:26
  134.9 0.0 all-reduce.5.cloned.1.call-update
  134.9 20.1 %all-reduce.5.cloned.1.call-done = f32[64,512]{1,0:T(8,128)} async-done(((f32[64,512]{1,0:T(8,128)}), f32[64,512]{1,0:T(8,128)}) %all-reduce.5.cloned.1.call-update) | async-done | bytes 131088 | tf_op jit(solution)/shard_map/psum | solution.py:31
  155.0 1.0 fusion
  156.0 11.7 %psum.39 = f32[64]{0:T(128)S(1)} all-reduce(f32[64]{0:T(128)S(1)} %fusion), channel_id=1, replica_groups=mesh['grp'=2,'ra'=4,'cb'=2,'dp'=2] {'ra'}, use_global_device_ids=true, to_apply=%region_9.10 | all-reduce | flops 64 | bytes 512 | tf_op jit(solution)/shard_map/psum | solution.py:12
  167.7 0.0 copy-done.2
  167.7 1.6 fusion.2
  (3 shorter events, 0.0 us)
Async XLA Ops:
  6.5 4.2 %copy-start = (bf16[64,512]{1,0:T(8,128)(2,1)S(1)}, bf16[64,512]{1,0:T(8,128)(2,1)}, u32[]{:S(2)}) copy-start(bf16[64,512]{1,0:T(8,128)(2,1)} %param.8) | copy-start | bytes 196612
  6.5 34.4 %reduce-scatter.3.cloned.1.call-start = ((), (), s32[]{:S(2)}) async-start(), calls=%async_computation.2 | async-start | bytes 1310720 | tf_op jit(solution)/shard_map/reduce_scatter | solution.py:24
  10.6 72.1 %copy-start.1 = (f32[512]{0:T(512)S(1)}, f32[512]{0:T(512)}, u32[]{:S(2)}) copy-start(f32[512]{0:T(512)} %param.12) | copy-start | bytes 6148
  10.7 71.0 %all-reduce.3.cloned.1.call-start = ((), (), s32[]{:S(2)}) async-start(), calls=%async_computation.3 | async-start | bytes 262144 | tf_op jit(solution)/shard_map/psum | solution.py:31
  61.5 52.7 %reduce-scatter.5.cloned.1.call-start = ((), (), s32[]{:S(2)}) async-start(), calls=%async_computation.4 | async-start | bytes 1310720 | tf_op jit(solution)/shard_map/reduce_scatter | solution.py:24
  86.7 81.0 %copy-start.2 = (f32[512]{0:T(512)S(1)}, f32[512]{0:T(512)}, u32[]{:S(2)}) copy-start(f32[512]{0:T(512)} %param.15) | copy-start | bytes 6148
  86.8 68.2 %all-reduce.5.cloned.1.call-start = ((), (), s32[]{:S(2)}) async-start(), calls=%async_computation.5 | async-start | bytes 262144 | tf_op jit(solution)/shard_map/psum | solution.py:31
Sparse Core Ops, SparseCore 0:
  10.8 30.0 reduce-scatter.2
  61.7 19.9 all-reduce.2
  86.9 27.3 reduce-scatter.4
  135.0 19.9 all-reduce.4
where the time goes:
time: 176 us
  waiting for transfers between devices  72.4 us (41%)
  blocking collectives  68.8 us (39%)
  matrix products  15.5 us (9%)
  between operations  13.2 us (8%)
  other arithmetic  5.91 us (3%)
    psum x2, waiting for transfers between devices, mlp_branch(): return lax.psum(down, 'cb')  40.2 us
    psum x3, blocking collectives, squares_inverse(): summed_sq = lax.psum(local_sq, 'ra')  37 us
    reduce_scatter x2, waiting for transfers between devices, mlp_branch(): lax.psum_scatter(partial_value, 'ra', scatter_dimension=1, tiled=True)  32.1 us
    all_gather x2, blocking collectives, mlp_branch(): lax.all_gather(hidden_share, 'ra', axis=1, tiled=True)  31.8 us
    dot_general x2, matrix products, mlp_branch(): partial_value = jnp.dot(scaled, w_up, preferred_element_type=jnp.float32)  8.13 us
    dot_general x2, matrix products, mlp_branch(): jnp.dot(lax.all_gather(hidden_share, 'ra', axis=1, tiled=True), w_down, p...  7.35 us
  transfers between devices with their start and end apart: 4, of which 4 were waited for; matrix products, arithmetic and copies ran while one was open for 0% of the time, Pallas kernels for 0%

commit v1 on v0

--- a/solution.py
+++ b/solution.py
@@ -9,7 +9,11 @@
 
 def squares_inverse(h32):
     local_sq = jnp.sum(h32 * h32, axis=1)
-    summed_sq = lax.psum(local_sq, "ra")
+    summed_sq = local_sq
+    for hop in (1, 2):
+        summed_sq = summed_sq + lax.ppermute(
+            summed_sq, "ra", [(dev, dev ^ hop) for dev in range(4)]
+        )
     return lax.rsqrt(summed_sq / D + EPS)
 
 

time: 176 us -> 173 us (0.983)
  blocking collectives: 68.8 us -> 31.9 us
  waiting for transfers between devices: 72.4 us -> 91.6 us
  starting transfers between devices: 0.13 us -> 14.2 us
    psum x3 -> x0, blocking collectives: 37 us -> none  [squares_inverse(): summed_sq = lax.psum(local_sq, 'ra')]
    ppermute x0 -> x6, starting transfers between devices: none -> 14.1 us  [squares_inverse(): lax.ppermute(summed_sq, 'ra', [(dev, dev ^ hop) for dev in range(4)])]
    ppermute x0 -> x6, waiting for transfers between devices: none -> 11.4 us  [squares_inverse(): lax.ppermute(summed_sq, 'ra', [(dev, dev ^ hop) for dev in range(4)])]
    reduce_scatter x2, waiting for transfers between devices: 32.1 us -> 40 us  [mlp_branch(): lax.psum_scatter(partial_value, 'ra', scatter_dimension=1, tiled=True)]
  transfers between devices with their start and end apart: 4 -> 10, of which waited for: 4 -> 10; matrix products, arithmetic and copies ran while one was open for 0% -> 0% of each run, Pallas kernels for 0% -> 0%
where the time goes in v1:
time: 173 us; the launch traced here: 172 us
  waiting for transfers between devices  91.6 us (53%)
  blocking collectives  31.9 us (18%)
  matrix products  15.4 us (9%)
  starting transfers between devices  14.2 us (8%)
  between operations  13.2 us (8%)
  other arithmetic  5.91 us (3%)
    psum x2, waiting for transfers between devices, mlp_branch(): return lax.psum(down, 'cb')  40.1 us
    reduce_scatter x2, waiting for transfers between devices, mlp_branch(): lax.psum_scatter(partial_value, 'ra', scatter_dimension=1, tiled=True)  40 us
    all_gather x2, blocking collectives, mlp_branch(): lax.all_gather(hidden_share, 'ra', axis=1, tiled=True)  31.9 us
    ppermute x6, starting transfers between devices, squares_inverse(): lax.ppermute(summed_sq, 'ra', [(dev, dev ^ hop) for dev in range(4)])  14.1 us
    ppermute x6, waiting for transfers between devices, squares_inverse(): lax.ppermute(summed_sq, 'ra', [(dev, dev ^ hop) for dev in range(4)])  11.4 us
    dot_general x2, matrix products, mlp_branch(): partial_value = jnp.dot(scaled, w_up, preferred_element_type=jnp.float32)  8.11 us
    dot_general x2, matrix products, mlp_branch(): jnp.dot(lax.all_gather(hidden_share, 'ra', axis=1, tiled=True), w_down, p...  7.34 us
  transfers between devices with their start and end apart: 10, of which 10 were waited for; matrix products, arithmetic and copies ran while one was open for 0% of the time, Pallas kernels for 0%

profile of v1, /device:TPU:0, one launch (start us, length us, event | category | flops | bytes accessed | tf_op | source)
XLA Modules:
  0.0 172.2 jit_solution(4120927856680298648)
XLA Ops:
  6.5 0.0 copy-start
  6.5 0.0 reduce-scatter.3.cloned.1.call-start
  6.5 4.1 %fusion.13 = f32[64,4096]{1,0:T(8,128)} fusion(bf16[512,4096]{1,0:T(8,128)(2,1)} %param.10, bf16[64,512]{1,0:T(8,128)(2,1)} %param.8, f32[512]{0:T(512)} %param.9), kind=kOutput, calls=%fused_computation.22 | convolution fusion | flops 268533760 | bytes 5310464 | tf_op jit(solution)/shard_map/dot_general | solution.py:26
  10.6 0.0 copy-start.1
  10.6 0.0 reduce-scatter.3.cloned.1.call-update
  10.7 0.0 all-reduce.3.cloned.1.call-start
  10.7 0.0 copy-done
  10.7 0.1 fusion.6
  10.8 3.1 %collective-permute-start = (f32[64]{0:T(128)S(1)}, f32[64]{0:T(128)S(1)}, u32[]{:S(2)}, u32[]{:S(2)}) collective-permute-start(f32[64]{0:T(128)S(1)} %fusion.6), channel_id=1, source_target_pairs={{0,4},{4,0},{8,12},{12,8},{1,5},{5,1},{9,13},{13,9},{2,6},{6,2},{1... | collective-permute-start | bytes 776 | tf_op jit(solution)/shard_map/ppermute | solution.py:14
  14.0 1.5 collective-permute-done
  15.5 3.0 %collective-permute-start.1 = (f32[64]{0:T(128)S(1)}, f32[64]{0:T(128)S(1)}, u32[]{:S(2)}, u32[]{:S(2)}) collective-permute-start(f32[64]{0:T(128)S(1)} %add.41), channel_id=1, source_target_pairs={{0,8},{4,12},{8,0},{12,4},{1,9},{5,13},{9,1},{13,5},{2,10},{6,14},... | collective-permute-start | bytes 776 | tf_op jit(solution)/shard_map/ppermute | solution.py:14
  18.5 1.5 collective-permute-done.1
  20.1 20.7 %reduce-scatter.3.cloned.1.call-done = f32[64,1024]{1,0:T(8,128)} async-done(((f32[64,4096]{1,0:T(8,128)}), f32[64,1024]{1,0:T(8,128)}) %reduce-scatter.3.cloned.1.call-update) | async-done | bytes 262160 | tf_op jit(solution)/shard_map/reduce_scatter | solution.py:28
  40.8 1.0 multiply_convert_fusion.1
  41.9 16.0 %all_gather.6 = bf16[64,4096]{1,0:T(8,128)(2,1)S(1)} all-gather(bf16[64,1024]{1,0:T(8,128)(2,1)S(1)} %multiply_convert_fusion.1), channel_id=1, replica_groups=mesh['grp'=2,'ra'=4,'cb'=2,'dp'=2] {'ra'}, dimensions={1}, use_global_device_ids=true | all-gather | bytes 655360 | tf_op jit(solution)/shard_map/all_gather | solution.py:31
  57.8 3.7 %fusion.18 = f32[64,512]{1,0:T(8,128)} fusion(bf16[64,4096]{1,0:T(8,128)(2,1)S(1)} %all_gather.6, bf16[4096,512]{1,0:T(8,128)(2,1)} %param.11), kind=kOutput, calls=%fused_computation.28 | convolution fusion | flops 268435456 | bytes 4849664 | tf_op jit(solution)/shard_map/dot_general | solution.py:30
  61.5 0.0 all-reduce.3.cloned.1.call-update
  61.5 0.0 reduce-scatter.5.cloned.1.call-start
  61.6 20.0 %all-reduce.3.cloned.1.call-done = f32[64,512]{1,0:T(8,128)} async-done(((f32[64,512]{1,0:T(8,128)}), f32[64,512]{1,0:T(8,128)}) %all-reduce.3.cloned.1.call-update) | async-done | bytes 131088 | tf_op jit(solution)/shard_map/psum | solution.py:35
  81.6 1.0 fusion.10
  82.6 0.0 copy-done.1
  82.6 4.0 %fusion.11 = f32[64,4096]{1,0:T(8,128)} fusion(bf16[512,4096]{1,0:T(8,128)(2,1)} %param.13, bf16[64,512]{1,0:T(8,128)(2,1)S(1)} %get-tuple-element.6, f32[512]{0:T(512)S(1)} %copy-done.1), kind=kOutput, calls=%fused_computation.21 | convolution fusion | flops 268533760 | bytes 5310464 | tf_op jit(solution)/shard_map/dot_general | solution.py:26
  86.6 0.0 copy-start.2
  86.6 0.0 reduce-scatter.5.cloned.1.call-update
  86.6 0.0 all-reduce.5.cloned.1.call-start
  86.7 1.6 collective-permute-start.2
  88.2 2.1 %collective-permute-done.2 = f32[64]{0:T(128)S(1)} collective-permute-done((f32[64]{0:T(128)S(1)}, f32[64]{0:T(128)S(1)}, u32[]{:S(2)}, u32[]{:S(2)}) %collective-permute-start.2) | collective-permute-done | bytes 288 | tf_op jit(solution)/shard_map/ppermute | solution.py:14
  90.3 2.4 %collective-permute-start.3 = (f32[64]{0:T(128)S(1)}, f32[64]{0:T(128)S(1)}, u32[]{:S(2)}, u32[]{:S(2)}) collective-permute-start(f32[64]{0:T(128)S(1)} %add.45), channel_id=1, source_target_pairs={{0,8},{4,12},{8,0},{12,4},{1,9},{5,13},{9,1},{13,5},{2,10},{6,14},... | collective-permute-start | bytes 776 | tf_op jit(solution)/shard_map/ppermute | solution.py:14
  92.7 2.1 %collective-permute-done.3 = f32[64]{0:T(128)S(1)} collective-permute-done((f32[64]{0:T(128)S(1)}, f32[64]{0:T(128)S(1)}, u32[]{:S(2)}, u32[]{:S(2)}) %collective-permute-start.3) | collective-permute-done | bytes 288 | tf_op jit(solution)/shard_map/ppermute | solution.py:14
  94.8 19.3 %reduce-scatter.5.cloned.1.call-done = f32[64,1024]{1,0:T(8,128)} async-done(((f32[64,4096]{1,0:T(8,128)}), f32[64,1024]{1,0:T(8,128)}) %reduce-scatter.5.cloned.1.call-update) | async-done | bytes 262160 | tf_op jit(solution)/shard_map/reduce_scatter | solution.py:28
  114.1 1.0 multiply_convert_fusion
  115.1 15.9 %all_gather.7 = bf16[64,4096]{1,0:T(8,128)(2,1)S(1)} all-gather(bf16[64,1024]{1,0:T(8,128)(2,1)S(1)} %multiply_convert_fusion), channel_id=1, replica_groups=mesh['grp'=2,'ra'=4,'cb'=2,'dp'=2] {'ra'}, dimensions={1}, use_global_device_ids=true | all-gather | bytes 655360 | tf_op jit(solution)/shard_map/all_gather | solution.py:31
  131.1 3.7 %fusion.19 = f32[64,512]{1,0:T(8,128)} fusion(bf16[64,4096]{1,0:T(8,128)(2,1)S(1)} %all_gather.7, bf16[4096,512]{1,0:T(8,128)(2,1)} %param.14), kind=kOutput, calls=%fused_computation.29 | convolution fusion | flops 268435456 | bytes 4849664 | tf_op jit(solution)/shard_map/dot_general | solution.py:30
  134.8 0.0 all-reduce.5.cloned.1.call-update
  134.8 20.1 %all-reduce.5.cloned.1.call-done = f32[64,512]{1,0:T(8,128)} async-done(((f32[64,512]{1,0:T(8,128)}), f32[64,512]{1,0:T(8,128)}) %all-reduce.5.cloned.1.call-update) | async-done | bytes 131088 | tf_op jit(solution)/shard_map/psum | solution.py:35
  154.9 1.0 fusion
  155.9 1.6 collective-permute-start.4
  157.5 2.1 %collective-permute-done.4 = f32[64]{0:T(128)S(1)} collective-permute-done((f32[64]{0:T(128)S(1)}, f32[64]{0:T(128)S(1)}, u32[]{:S(2)}, u32[]{:S(2)}) %collective-permute-start.4) | collective-permute-done | bytes 288 | tf_op jit(solution)/shard_map/ppermute | solution.py:14
  159.6 2.4 %collective-permute-start.5 = (f32[64]{0:T(128)S(1)}, f32[64]{0:T(128)S(1)}, u32[]{:S(2)}, u32[]{:S(2)}) collective-permute-start(f32[64]{0:T(128)S(1)} %add.49), channel_id=1, source_target_pairs={{0,8},{4,12},{8,0},{12,4},{1,9},{5,13},{9,1},{13,5},{2,10},{6,14},... | collective-permute-start | bytes 776 | tf_op jit(solution)/shard_map/ppermute | solution.py:14
  162.0 2.1 %collective-permute-done.5 = f32[64]{0:T(128)S(1)} collective-permute-done((f32[64]{0:T(128)S(1)}, f32[64]{0:T(128)S(1)}, u32[]{:S(2)}, u32[]{:S(2)}) %collective-permute-start.5) | collective-permute-done | bytes 288 | tf_op jit(solution)/shard_map/ppermute | solution.py:14
  164.0 0.0 copy-done.2
  164.0 1.6 fusion.2
  (6 shorter events, 0.0 us)
Async XLA Ops:
  6.5 4.2 %copy-start = (bf16[64,512]{1,0:T(8,128)(2,1)S(1)}, bf16[64,512]{1,0:T(8,128)(2,1)}, u32[]{:S(2)}) copy-start(bf16[64,512]{1,0:T(8,128)(2,1)} %param.8) | copy-start | bytes 196612
  6.5 34.3 %reduce-scatter.3.cloned.1.call-start = ((), (), s32[]{:S(2)}) async-start(), calls=%async_computation.2 | async-start | bytes 1310720 | tf_op jit(solution)/shard_map/reduce_scatter | solution.py:28
  10.6 72.0 %copy-start.1 = (f32[512]{0:T(512)S(1)}, f32[512]{0:T(512)}, u32[]{:S(2)}) copy-start(f32[512]{0:T(512)} %param.12) | copy-start | bytes 6148
  10.7 70.9 %all-reduce.3.cloned.1.call-start = ((), (), s32[]{:S(2)}) async-start(), calls=%async_computation.3 | async-start | bytes 262144 | tf_op jit(solution)/shard_map/psum | solution.py:35
  10.8 4.7 %collective-permute-start = (f32[64]{0:T(128)S(1)}, f32[64]{0:T(128)S(1)}, u32[]{:S(2)}, u32[]{:S(2)}) collective-permute-start(f32[64]{0:T(128)S(1)} %fusion.6), channel_id=1, source_target_pairs={{0,4},{4,0},{8,12},{12,8},{1,5},{5,1},{9,13},{13,9},{2,6},{6,2},{1... | collective-permute-start | bytes 776 | tf_op jit(solution)/shard_map/ppermute | solution.py:14
  15.5 4.6 %collective-permute-start.1 = (f32[64]{0:T(128)S(1)}, f32[64]{0:T(128)S(1)}, u32[]{:S(2)}, u32[]{:S(2)}) collective-permute-start(f32[64]{0:T(128)S(1)} %add.41), channel_id=1, source_target_pairs={{0,8},{4,12},{8,0},{12,4},{1,9},{5,13},{9,1},{13,5},{2,10},{6,14},... | collective-permute-start | bytes 776 | tf_op jit(solution)/shard_map/ppermute | solution.py:14
  61.5 52.6 %reduce-scatter.5.cloned.1.call-start = ((), (), s32[]{:S(2)}) async-start(), calls=%async_computation.4 | async-start | bytes 1310720 | tf_op jit(solution)/shard_map/reduce_scatter | solution.py:28
  86.6 77.4 %copy-start.2 = (f32[512]{0:T(512)S(1)}, f32[512]{0:T(512)}, u32[]{:S(2)}) copy-start(f32[512]{0:T(512)} %param.15) | copy-start | bytes 6148
  86.6 68.2 %all-reduce.5.cloned.1.call-start = ((), (), s32[]{:S(2)}) async-start(), calls=%async_computation.5 | async-start | bytes 262144 | tf_op jit(solution)/shard_map/psum | solution.py:35
  86.7 3.6 %collective-permute-start.2 = (f32[64]{0:T(128)S(1)}, f32[64]{0:T(128)S(1)}, u32[]{:S(2)}, u32[]{:S(2)}) collective-permute-start(f32[64]{0:T(128)S(1)} %get-tuple-element.5), channel_id=1, source_target_pairs={{0,4},{4,0},{8,12},{12,8},{1,5},{5,1},{9,13},{13,9},{2,6},{6,2},{1... | collective-permute-start | bytes 776 | tf_op jit(solution)/shard_map/ppermute | solution.py:14
  90.3 4.5 %collective-permute-start.3 = (f32[64]{0:T(128)S(1)}, f32[64]{0:T(128)S(1)}, u32[]{:S(2)}, u32[]{:S(2)}) collective-permute-start(f32[64]{0:T(128)S(1)} %add.45), channel_id=1, source_target_pairs={{0,8},{4,12},{8,0},{12,4},{1,9},{5,13},{9,1},{13,5},{2,10},{6,14},... | collective-permute-start | bytes 776 | tf_op jit(solution)/shard_map/ppermute | solution.py:14
  155.9 3.6 %collective-permute-start.4 = (f32[64]{0:T(128)S(1)}, f32[64]{0:T(128)S(1)}, u32[]{:S(2)}, u32[]{:S(2)}) collective-permute-start(f32[64]{0:T(128)S(1)} %fusion), channel_id=1, source_target_pairs={{0,4},{4,0},{8,12},{12,8},{1,5},{5,1},{9,13},{13,9},{2,6},{6,2},{1... | collective-permute-start | bytes 776 | tf_op jit(solution)/shard_map/ppermute | solution.py:14
  159.6 4.5 %collective-permute-start.5 = (f32[64]{0:T(128)S(1)}, f32[64]{0:T(128)S(1)}, u32[]{:S(2)}, u32[]{:S(2)}) collective-permute-start(f32[64]{0:T(128)S(1)} %add.49), channel_id=1, source_target_pairs={{0,8},{4,12},{8,0},{12,4},{1,9},{5,13},{9,1},{13,5},{2,10},{6,14},... | collective-permute-start | bytes 776 | tf_op jit(solution)/shard_map/ppermute | solution.py:14
Sparse Core Ops, SparseCore 0:
  10.8 29.9 reduce-scatter.2
  61.6 19.8 all-reduce.2
  86.8 27.2 reduce-scatter.4
  134.9 19.9 all-reduce.4
